TPU v7x, 32 devices: a whole 2x2x4 slice. The times are simulated.
32 devices in a mesh: sp: 16 (over z, y, x), tp: 2 (over core).
Axes of the slice: x: 2, y: 2, z: 4, core: 2. Of those that a mesh axis runs over, the one named last changes fastest.
Arguments:
- features: bfloat16 [4096, 1024], P('sp', 'tp'), may hold values from -6 to 6
- lambda_real: float32 [64, 64], P('tp'), may hold values from -4 to 0, as said below
- lambda_imag: float32 [64, 64], P('tp'), may hold values from 0.5 to 201.06177
- log_step: float32 [64], P('tp'), may hold values from -5 to -2
- input_real: float32 [64, 64, 16], P('tp'), may hold values from -2 to 2
- input_imag: float32 [64, 64, 16], P('tp'), may hold values from -2 to 2
- real_output: float32 [64, 16, 64], P('tp'), may hold values from -0.75 to 0.75
- imaginary_output: float32 [64, 16, 64], P('tp'), may hold values from -0.75 to 0.75
- skip_gain: float32 [1024], P('tp'), may hold values from -4 to 4
- value_weight: bfloat16 [1024, 2048], P('tp'), may hold values from -0.1875 to 0.1875
- gate_weight: bfloat16 [1024, 2048], P('tp'), may hold values from -0.1875 to 0.1875
- value_bias: float32 [2048], replicated, may hold values from -3 to 3
- gate_bias: float32 [2048], replicated, may hold values from -3 to 3
Outputs:
- mixed_output: bfloat16 [4096, 2048], P(('sp', 'tp'))
Inputs may be any that keep to these rules, and one draw needn't show every extreme that they name: `lambda_real`: negative.
All inputs are finite; a program needn't handle non-finite values.
Results may differ from a plain program's by a relative error of at most 0.03.
Values may be sent and summed in bfloat16 or wider, within the bound.
A program may use at most 128 MiB of HBM per device.

v0:
```python
import math
import jax
import jax.numpy as jnp
from jax import lax
from jax.sharding import PartitionSpec as P


def prefix(part, axis, combine, identity):
    place = lax.axis_index(axis)
    gathered = jax.tree.map(lambda a: lax.all_gather(a, axis), part)
    state = jax.tree.map(lambda a, e: jnp.zeros_like(a) + jnp.asarray(e, a.dtype), part, identity)

    def one(lap, state):
        return combine(
            state, jax.tree.map(lambda a: lax.dynamic_index_in_dim(a, lap, 0, False), gathered)
        )

    return lax.fori_loop(0, place, one, state)


def discretize(lambda_real, lambda_imag, log_step, input_real, input_imag):
    step_size = jnp.exp(log_step)[:, None]
    magnitude = jnp.exp(lambda_real * step_size)
    phase_arg = lambda_imag * step_size
    trans_re = magnitude * jnp.cos(phase_arg)
    trans_im = magnitude * jnp.sin(phase_arg)
    denominator = lambda_real * lambda_real + lambda_imag * lambda_imag
    num_re = trans_re - 1.0
    f_re = (num_re * lambda_real + trans_im * lambda_imag) / denominator
    f_im = (trans_im * lambda_real - num_re * lambda_imag) / denominator
    bar_re = f_re[..., None] * input_real - f_im[..., None] * input_imag
    bar_im = f_re[..., None] * input_imag + f_im[..., None] * input_real
    return (step_size, bar_re, bar_im)


def powers_flat(lambda_real, lambda_imag, step_size, first, count):
    exponent = (jnp.arange(count, dtype=jnp.int32) + first).astype(jnp.float32)[:, None]
    rate_re = (lambda_real * step_size).reshape(1, -1)
    rate_im = (lambda_imag * step_size).reshape(1, -1)
    magnitude = jnp.exp(exponent * rate_re)
    phase_arg = exponent * rate_im
    return (magnitude * jnp.cos(phase_arg), magnitude * jnp.sin(phase_arg))


def combine(earlier, later):
    a1r, a1i, b1r, b1i = earlier
    a2r, a2i, b2r, b2i = later
    return (
        a1r * a2r - a1i * a2i,
        a1r * a2i + a1i * a2r,
        a2r * b1r - a2i * b1i + b2r,
        a2r * b1i + a2i * b1r + b2i,
    )


def within_blocks(step_re, step_im, bu_re, bu_im, span):
    blocks_re = bu_re.reshape(-1, span, bu_re.shape[1])
    blocks_im = bu_im.reshape(-1, span, bu_im.shape[1])
    h_re = jnp.zeros_like(blocks_re[:, 0])
    h_im = jnp.zeros_like(blocks_im[:, 0])
    rows_re = []
    rows_im = []
    for offset in range(span):
        new_re = step_re * h_re - step_im * h_im + blocks_re[:, offset]
        new_im = step_re * h_im + step_im * h_re + blocks_im[:, offset]
        h_re, h_im = (new_re, new_im)
        rows_re.append(h_re)
        rows_im.append(h_im)
    return (jnp.stack(rows_re, axis=1), jnp.stack(rows_im, axis=1))


def block_carries(span_re, span_im, ends_re, ends_im, start_re, start_im):

    def advance(carried, ends):
        c_re, c_im = carried
        e_re, e_im = ends
        next_re = span_re * c_re - span_im * c_im + e_re
        next_im = span_re * c_im + span_im * c_re + e_im
        return ((next_re, next_im), (c_re, c_im))

    final, entering = lax.scan(advance, (start_re, start_im), (ends_re, ends_im))
    return (final, entering)


def local(
    features,
    lambda_real,
    lambda_imag,
    log_step,
    input_real,
    input_imag,
    real_output,
    imaginary_output,
    skip_gain,
    value_weight,
    gate_weight,
    value_bias,
    gate_bias,
):
    upper_limit = lax.Precision.HIGHEST
    positions = features.shape[0]
    groups = lambda_real.shape[0]
    state_width = lambda_real.shape[1]
    group_size = input_real.shape[2]
    flat_width = groups * state_width
    span = math.gcd(positions, 16)
    step_size, bar_re, bar_im = discretize(
        lambda_real, lambda_imag, log_step, input_real, input_imag
    )
    inner_re, inner_im = powers_flat(lambda_real, lambda_imag, step_size, 1, span)
    whole_re, whole_im = powers_flat(lambda_real, lambda_imag, step_size, positions, 1)
    step_re, step_im = (inner_re[0], inner_im[0])
    span_re, span_im = (inner_re[-1], inner_im[-1])
    widened = features.astype(jnp.float32)
    grouped = widened.reshape(positions, groups, group_size)
    bu_re = jnp.einsum("sgc,gpc->sgp", grouped, bar_re, precision=upper_limit).reshape(
        positions, flat_width
    )
    bu_im = jnp.einsum("sgc,gpc->sgp", grouped, bar_im, precision=upper_limit).reshape(
        positions, flat_width
    )
    local_re, local_im = within_blocks(step_re, step_im, bu_re, bu_im, span)
    ends_re, ends_im = (local_re[:, -1], local_im[:, -1])
    zero_state = jnp.zeros((flat_width,), jnp.float32)
    ones_state = jnp.ones((flat_width,), jnp.float32)
    identity = (ones_state, zero_state, zero_state, zero_state)
    final, entering = block_carries(span_re, span_im, ends_re, ends_im, zero_state, zero_state)
    enter_re = entering[0][:, None]
    enter_im = entering[1][:, None]
    signal_real = local_re + inner_re * enter_re - inner_im * enter_im
    signal_imaginary = local_im + inner_re * enter_im + inner_im * enter_re
    signal_real = signal_real.reshape(positions, flat_width)
    signal_imaginary = signal_imaginary.reshape(positions, flat_width)
    incoming = prefix((whole_re[0], whole_im[0], final[0], final[1]), "sp", combine, identity)
    h_re, h_im = (incoming[2], incoming[3])
    all_re, all_im = powers_flat(lambda_real, lambda_imag, step_size, 1, positions)
    signal_real = signal_real + all_re * h_re - all_im * h_im
    signal_imaginary = signal_imaginary + all_re * h_im + all_im * h_re
    signal_real = signal_real.reshape(positions, groups, state_width)
    signal_imaginary = signal_imaginary.reshape(positions, groups, state_width)
    mixer_response = jnp.einsum(
        "qej,eoj->qeo", signal_real, real_output, precision=upper_limit
    ) - jnp.einsum("qej,eoj->qeo", signal_imaginary, imaginary_output, precision=upper_limit)
    mixer_response = mixer_response.reshape(positions, groups * group_size) + skip_gain * widened
    activated = jax.nn.gelu(mixer_response).astype(jnp.bfloat16)
    model_width = value_weight.shape[1]
    moved = lax.all_to_all(activated, "tp", split_axis=0, concat_axis=1, tiled=True)
    full_value, full_gate = (
        lax.all_gather(value_weight, "tp", axis=0, tiled=True),
        lax.all_gather(gate_weight, "tp", axis=0, tiled=True),
    )
    pieces = lax.axis_size("tp")
    row_total = moved.shape[0]
    slice_width = value_weight.shape[0]
    blocks_act = moved.reshape(row_total, pieces, slice_width)

    def halves(weight):
        partial_value = jnp.einsum(
            "rnc,ncd->nrd",
            blocks_act,
            weight.reshape(pieces, slice_width, model_width),
            preferred_element_type=jnp.float32,
        )
        rounded = lax.optimization_barrier(partial_value.astype(jnp.bfloat16))
        return jnp.sum(rounded.astype(jnp.float32), axis=0)

    value_sum = halves(full_value)
    gate_sum = halves(full_gate)
    value_sum = value_sum + value_bias
    gate_sum = gate_sum + gate_bias
    return (value_sum * jax.nn.sigmoid(gate_sum)).astype(jnp.bfloat16)


def solution(mesh):
    in_specs = (
        P("sp", "tp"),
        P("tp", None),
        P("tp", None),
        P("tp"),
        P("tp", None, None),
        P("tp", None, None),
        P("tp", None, None),
        P("tp", None, None),
        P("tp"),
        P("tp", None),
        P("tp", None),
        P(),
        P(),
    )
    out_specs = P(("sp", "tp"), None)
    return jax.shard_map(local, mesh=mesh, in_specs=in_specs, out_specs=out_specs, check_vma=False)
```

profile of v0, /device:TPU:31, one launch (start us, length us, event | category | flops | bytes accessed | tf_op | source)
XLA Modules:
  0.0 345.9 jit_solution(2314690990529979079)
XLA Ops:
  9.6 2.4 convolution_bitcast_fusion.1
  14.4 6.1 %copy.90 = f32[256,32,64]{2,1,0:T(8,128)} copy(f32[256,32,64]{0,2,1:T(8,128)} %convolution_bitcast_fusion.1) | data formatting | bytes 4194304 | tf_op jit(solution)/shard_map/sgc,gpc->sgp/transpose | solution.py:116
  20.4 5.1 %reshape_reshape.6 = f32[16,16,2048]{2,1,0:T(8,128)} reshape(f32[256,32,64]{2,1,0:T(8,128)} %copy.90) | data formatting | bytes 4194304 | tf_op jit(solution)/shard_map/reshape;reshape | solution.py:57
  25.5 9.8 %fusion.35 = (f32[16,1,2048]{2,1,0:T(1,128)}, f32[16,1,2048]{2,1,0:T(1,128)S(1)}, f32[16,1,2048]{2,1,0:T(1,128)}, f32[16,1,2048]{2,1,0:T(1,128)}, f32[16,1,2048]...) fusion(f32[16,16,2048]{2,1,0:T(8,128)} %reshape_reshape.6), kind=kLoop, calls=%fused_computation.170 | loop fusion | bytes 4194304 | tf_op jit(solution)/shard_map/slice | solution.py:64
  35.3 4.5 %copy.92 = f32[256,32,64]{2,1,0:T(8,128)} copy(f32[256,32,64]{0,2,1:T(8,128)S(1)} %convolution_bitcast_fusion) | data formatting | bytes 4194304 | tf_op jit(solution)/shard_map/sgc,gpc->sgp/transpose | solution.py:119
  39.8 3.6 %reshape_reshape.7 = f32[16,16,2048]{2,1,0:T(8,128)S(1)} reshape(f32[256,32,64]{2,1,0:T(8,128)} %copy.92) | data formatting | bytes 4194304 | tf_op jit(solution)/shard_map/reshape;reshape | solution.py:58
  43.5 1.6 fusion.34
  48.9 48.8 %while.33 = (s32[]{:T(128)}, f32[2048]{0:T(1024)S(1)}, f32[2048]{0:T(1024)S(1)}, f32[16,2048]{1,0:T(8,128)}, f32[16,2048]{1,0:T(8,128)}, /*index=5*/f32[2048]{0:...) while((s32[]{:T(128)}, f32[2048]{0:T(1024)S(1)}, ...), condition=%wide.region_1.2_spmd.clone, body=%wide.region_0.1_spmd.clone.sunk | while | flops 20483 | bytes 180355 | solution.py:81
  97.7 29.1 %all-gather = f32[32768]{0:T(1024)S(1)} all-gather(f32[2048]{0:T(1024)S(1)} %get-tuple-element.127), channel_id=2, replica_groups=mesh['sp'=16,'tp'=2] {'sp'}, dimensions={0}, use_global_device_ids=true | all-gather | bytes 139264 | tf_op jit(solution)/shard_map/all_gather | solution.py:10
  126.9 31.3 %all-gather.1 = f32[32768]{0:T(1024)S(1)} all-gather(f32[2048]{0:T(1024)S(1)} %get-tuple-element.128), channel_id=3, replica_groups=mesh['sp'=16,'tp'=2] {'sp'}, dimensions={0}, use_global_device_ids=true | all-gather | bytes 139264 | tf_op jit(solution)/shard_map/all_gather | solution.py:10
  158.3 29.5 %all-gather.3 = f32[16,1,2048]{2,1,0:T(1,128)S(1)} all-gather(f32[1,1,2048]{2,1,0:T(1,128)S(1)} %reshape.5975), channel_id=1, replica_groups=mesh['sp'=16,'tp'=2] {'sp'}, dimensions={0}, use_global_device_ids=true | all-gather | bytes 139264 | tf_op jit(solution)/shard_map/all_gather | solution.py:10
  188.6 30.9 %all-gather.2 = f32[16,1,2048]{2,1,0:T(1,128)S(1)} all-gather(f32[1,1,2048]{2,1,0:T(1,128)S(1)} %reshape.5973), channel_id=1, replica_groups=mesh['sp'=16,'tp'=2] {'sp'}, dimensions={0}, use_global_device_ids=true | all-gather | bytes 139264 | tf_op jit(solution)/shard_map/all_gather | solution.py:10
  220.2 14.7 %while.32 = (s32[]{:T(128)}, f32[2048]{0:T(1024)S(1)}, f32[2048]{0:T(1024)S(1)}, s32[]{:T(128)}, f32[16,2048]{1,0:T(8,128)}, /*index=5*/f32[16,2048]{1,0:T(8,128...) while((s32[]{:T(128)}, f32[2048]{0:T(1024)S(1)}, ...), condition=%wide.region_3.4_spmd, body=%wide.region_2.3_spmd.sunk | while | flops 16389 | bytes 131223 | solution.py:18
  249.0 2.8 multiply_subtract_fusion.1
  251.9 2.5 copy.126
  254.4 4.9 %add.1212 = f32[256,32,64]{2,1,0:T(8,128)} reshape(f32[16,16,2048]{2,1,0:T(8,128)} %copy.126) | data formatting | bytes 4194304 | tf_op jit(solution)/shard_map/add | solution.py:131
  259.3 2.5 copy.124
  261.8 4.9 %sub.375 = f32[256,32,64]{2,1,0:T(8,128)} reshape(f32[16,16,2048]{2,1,0:T(8,128)} %copy.124) | data formatting | bytes 4194304 | tf_op jit(solution)/shard_map/sub | solution.py:130
  266.7 19.2 %multiply_subtract_fusion = (f32[256,32,64]{2,1,0:T(8,128)S(1)}, f32[256,32,64]{2,1,0:T(8,128)S(1)}) fusion(f32[256,32,64]{2,1,0:T(8,128)} %sub.375, f32[32,64]{1,0:T(8,128)S(1)} %mul.2004, f32[32,64]{1,0:T(8,128)S(1)} %mul.2000, f32[32,64]{1,0:T(8,128)S(1)} %copy-done.52, f32[32,64]{1,0:T(8,128)S(1)} %copy-done.54, f32[256]{0:T(256)S(1)} %add_convert_fusion, ...), kind=kLoop, calls=%fused_computation.21 | loop fusion | flops 6291456 | bytes 8422400 | tf_op jit(solution)/shard_map/sub | solution.py:137
  285.9 6.1 %fusion.2 = f32[32,256,16]{1,2,0:T(8,128)S(1)} fusion(f32[32,16,64]{2,1,0:T(8,128)S(1)} %copy-done, f32[256,32,64]{2,1,0:T(8,128)S(1)} %get-tuple-element.313), kind=kOutput, calls=%fused_computation.16 | convolution fusion | flops 100663296 | bytes 2752512 | tf_op jit(solution)/shard_map/qej,eoj->qeo/dot_general | solution.py:143
  292.1 6.1 %fusion.6 = f32[32,256,16]{1,2,0:T(8,128)S(1)} fusion(f32[32,256,16]{1,2,0:T(8,128)S(1)} %fusion.2, f32[32,16,64]{2,1,0:T(8,128)S(1)} %copy-done.50, f32[256,32,64]{2,1,0:T(8,128)S(1)} %get-tuple-element.312), kind=kOutput, calls=%fused_computation.31 | convolution fusion | flops 100794368 | bytes 3276800 | tf_op jit(solution)/shard_map/qej,eoj->qeo/dot_general | solution.py:141
  298.6 32.4 %all_to_all.16 = bf16[2,128,512]{2,1,0:T(8,128)(2,1)S(1)} all-to-all(bf16[2,128,512]{2,1,0:T(8,128)(2,1)S(1)} %bitcast.277), channel_id=1, replica_groups=mesh['sp'=16,'tp'=2] {'tp'}, dimensions={0} | all-to-all | bytes 524288 | tf_op jit(solution)/shard_map/all_to_all | solution.py:147
  331.0 2.9 convolution_convert_fusion.1
  334.1 2.9 convolution_convert_fusion
  (320 shorter events, 89.2 us)
Async XLA Ops:
  6.5 279.4 %copy-start = (f32[32,16,64]{2,1,0:T(8,128)S(1)}, f32[32,16,64]{2,1,0:T(8,128)}, u32[]{:S(2)}) copy-start(f32[32,16,64]{2,1,0:T(8,128)} %param.24) | copy-start | bytes 393220
  6.6 324.4 %all-gather.7.cloned.1.call-start = ((), (), s32[]{:S(2)}) async-start(), calls=%async_computation.1 | async-start | bytes 6291456 | tf_op jit(solution)/shard_map/all_gather | solution.py:149
  7.3 326.8 %all-gather.9.cloned.1.call-start = ((), (), s32[]{:S(2)}) async-start(), calls=%async_computation.2 | async-start | bytes 6291456 | tf_op jit(solution)/shard_map/all_gather | solution.py:150
  9.6 3.4 copy-start.53
  9.6 4.1 %copy-start.51 = (f32[32,64]{1,0:T(8,128)}, f32[32,64]{1,0:T(8,128)S(1)}, u32[]{:S(2)}) copy-start(f32[32,64]{1,0:T(8,128)S(1)} %get-tuple-element.318) | copy-start | bytes 24580
  43.5 3.5 %copy-start.15 = (f32[16,1,2048]{2,1,0:T(1,128)S(1)}, f32[16,1,2048]{2,1,0:T(1,128)}, u32[]{:S(2)}) copy-start(f32[16,1,2048]{2,1,0:T(1,128)} %get-tuple-element.281) | copy-start | bytes 393220
  43.5 3.5 %copy-start.19 = (f32[16,1,2048]{2,1,0:T(1,128)S(1)}, f32[16,1,2048]{2,1,0:T(1,128)}, u32[]{:S(2)}) copy-start(f32[16,1,2048]{2,1,0:T(1,128)} %get-tuple-element.283) | copy-start | bytes 393220
  43.5 3.5 %copy-start.23 = (f32[16,1,2048]{2,1,0:T(1,128)S(1)}, f32[16,1,2048]{2,1,0:T(1,128)}, u32[]{:S(2)}) copy-start(f32[16,1,2048]{2,1,0:T(1,128)} %get-tuple-element.284) | copy-start | bytes 393220
  48.1 110.1 %copy-start.58 = (f32[32,64]{1,0:T(8,128)S(1)}, f32[32,64]{1,0:T(8,128)}, u32[]{:S(2)}) copy-start(f32[32,64]{1,0:T(8,128)} %get-tuple-element.314) | copy-start | bytes 24580
  48.7 139.8 %copy-start.57 = (f32[32,64]{1,0:T(8,128)S(1)}, f32[32,64]{1,0:T(8,128)}, u32[]{:S(2)}) copy-start(f32[32,64]{1,0:T(8,128)} %get-tuple-element.315) | copy-start | bytes 24580
  48.9 186.0 %copy-start.41 = (f32[16,1,2048]{2,1,0:T(1,128)S(1)}, f32[16,1,2048]{2,1,0:T(1,128)}, u32[]{:S(2)}) copy-start(f32[16,1,2048]{2,1,0:T(1,128)} %get-tuple-element.287) | copy-start | bytes 393220
  48.9 186.8 %copy-start.35 = (f32[16,1,2048]{2,1,0:T(1,128)S(1)}, f32[16,1,2048]{2,1,0:T(1,128)}, u32[]{:S(2)}) copy-start(f32[16,1,2048]{2,1,0:T(1,128)} %get-tuple-element.286) | copy-start | bytes 393220
  48.9 186.8 %copy-start.39 = (f32[16,1,2048]{2,1,0:T(1,128)S(1)}, f32[16,1,2048]{2,1,0:T(1,128)}, u32[]{:S(2)}) copy-start(f32[16,1,2048]{2,1,0:T(1,128)} %copy-done.38) | copy-start | bytes 393220
  126.9 109.8 %copy-start.31 = (f32[16,1,2048]{2,1,0:T(1,128)S(1)}, f32[16,1,2048]{2,1,0:T(1,128)}, u32[]{:S(2)}) copy-start(f32[16,1,2048]{2,1,0:T(1,128)} %get-tuple-element.285) | copy-start | bytes 393220
  126.9 109.8 %copy-start.37 = (f32[16,1,2048]{2,1,0:T(1,128)S(1)}, f32[16,1,2048]{2,1,0:T(1,128)}, u32[]{:S(2)}) copy-start(f32[16,1,2048]{2,1,0:T(1,128)} %copy-done.36) | copy-start | bytes 393220
  220.2 17.3 %copy-start.24 = (f32[16,1,2048]{2,1,0:T(1,128)S(1)}, f32[16,1,2048]{2,1,0:T(1,128)}, u32[]{:S(2)}) copy-start(f32[16,1,2048]{2,1,0:T(1,128)} %get-tuple-element.284) | copy-start | bytes 393220
  220.2 17.3 %copy-start.33 = (f32[16,1,2048]{2,1,0:T(1,128)S(1)}, f32[16,1,2048]{2,1,0:T(1,128)}, u32[]{:S(2)}) copy-start(f32[16,1,2048]{2,1,0:T(1,128)} %copy-done.32) | copy-start | bytes 393220
  245.0 4.0 %copy-start.47 = (f32[16,2048]{1,0:T(8,128)S(1)}, f32[16,2048]{1,0:T(8,128)}, u32[]{:S(2)}) copy-start(f32[16,2048]{1,0:T(8,128)} %copy-done.46) | copy-start | bytes 393220
  245.0 4.0 %copy-start.49 = (f32[16,2048]{1,0:T(8,128)S(1)}, f32[16,2048]{1,0:T(8,128)}, u32[]{:S(2)}) copy-start(f32[16,2048]{1,0:T(8,128)} %copy-done.48) | copy-start | bytes 393220
  261.8 4.9 %copy-start.52 = (f32[32,64]{1,0:T(8,128)S(1)}, f32[32,64]{1,0:T(8,128)}, u32[]{:S(2)}) copy-start(f32[32,64]{1,0:T(8,128)} %copy-done.51) | copy-start | bytes 24580
  261.8 4.9 %copy-start.54 = (f32[32,64]{1,0:T(8,128)S(1)}, f32[32,64]{1,0:T(8,128)}, u32[]{:S(2)}) copy-start(f32[32,64]{1,0:T(8,128)} %copy-done.53) | copy-start | bytes 24580
  285.9 6.1 %copy-start.50 = (f32[32,16,64]{2,1,0:T(8,128)S(1)}, f32[32,16,64]{2,1,0:T(8,128)}, u32[]{:S(2)}) copy-start(f32[32,16,64]{2,1,0:T(8,128)} %param.23) | copy-start | bytes 393220
  292.0 6.3 %copy-start.45 = (bf16[256,512]{1,0:T(8,128)(2,1)S(1)}, bf16[256,512]{1,0:T(8,128)(2,1)}, u32[]{:S(2)}) copy-start(bf16[256,512]{1,0:T(8,128)(2,1)} %param.17) | copy-start | bytes 786436
  292.0 6.3 %copy-start.65 = (f32[512]{0:T(512)S(1)}, f32[512]{0:T(512)}, u32[]{:S(2)}) copy-start(f32[512]{0:T(512)} %param.25) | copy-start | bytes 6148
  (46 other events, 112.8 us)
Sparse Core Ops, SparseCore 0:
  8.9 15.2 all-gather.6
  25.8 14.8 all-gather.8
where the time goes:
time: 351 us; the launch traced here: 346 us
  blocking collectives  153 us (44%)
  local copies, waits for them, and re-layouts  112 us (32%)
  other arithmetic  41.9 us (12%)
  matrix products  21.4 us (6%)
  between operations  14.5 us (4%)
    all_gather x4, blocking collectives, prefix(): gathered = jax.tree.map(lambda a: lax.all_gather(a, axis), part)  121 us
    dynamic_update_slice x32, local copies, waits for them, and re-layouts, block_carries(): lax.scan(advance, (start_re, start_im), (ends_re, ends_im))  47.9 us
    all_to_all x1, blocking collectives, local(): lax.all_to_all(activated, 'tp', split_axis=0, concat_axis=1, tiled=True)  32.4 us
    sub x1, other arithmetic, local(): signal_real = signal_real + all_re * h_re - all_im * h_im  19.2 us
    dynamic_slice x30, local copies, waits for them, and re-layouts, one(): lax.dynamic_index_in_dim(a, lap, 0, False)  13.7 us
    unnamed x17, other arithmetic  12.3 us
    slice x1, local copies, waits for them, and re-layouts, within_blocks(): new_re = step_re * h_re - step_im * h_im + blocks_re[:, offset]  9.78 us
    sub x2, local copies, waits for them, and re-layouts, local(): signal_real = local_re + inner_re * enter_re - inner_im * enter_im  7.42 us
  transfers between devices with their start and end apart: 2, of which 0 were waited for; matrix products, arithmetic and copies ran while one was open for 49% of the time, Pallas kernels for 0%

commit v1 on v0

--- a/solution.py
+++ b/solution.py
@@ -1,8 +1,20 @@
+import functools
 import math
 import jax
 import jax.numpy as jnp
 from jax import lax
 from jax.sharding import PartitionSpec as P
+
+
+def _apply_forms(array_in, peer_axis, dim_at, along_dim):
+    frame_out = jax.lax.axis_size(peer_axis)
+    outcome_arr = jnp.split(array_in, frame_out, dim_at)
+    piece_next = jnp.stack(outcome_arr)
+    placed = jax.lax.all_to_all(piece_next, peer_axis, 0, 0)
+    return jnp.concatenate(placed, axis=along_dim)
+
+
+derive_bands_over_axis = functools.partial(_apply_forms, peer_axis="tp", dim_at=0, along_dim=1)
 
 
 def prefix(part, axis, combine, identity):
@@ -144,7 +156,7 @@
     mixer_response = mixer_response.reshape(positions, groups * group_size) + skip_gain * widened
     activated = jax.nn.gelu(mixer_response).astype(jnp.bfloat16)
     model_width = value_weight.shape[1]
-    moved = lax.all_to_all(activated, "tp", split_axis=0, concat_axis=1, tiled=True)
+    moved = derive_bands_over_axis(activated)
     full_value, full_gate = (
         lax.all_gather(value_weight, "tp", axis=0, tiled=True),
         lax.all_gather(gate_weight, "tp", axis=0, tiled=True),

time: 351 us -> 351 us (level)
  no operation moved by 1% of the time
where the time goes in v1:
time: 351 us; the launch traced here: 346 us
  blocking collectives  153 us (44%)
  local copies, waits for them, and re-layouts  112 us (32%)
  other arithmetic  41.9 us (12%)
  matrix products  21.4 us (6%)
  between operations  14.5 us (4%)
    all_gather x4, blocking collectives, prefix(): gathered = jax.tree.map(lambda a: lax.all_gather(a, axis), part)  120 us
    dynamic_update_slice x32, local copies, waits for them, and re-layouts, block_carries(): lax.scan(advance, (start_re, start_im), (ends_re, ends_im))  47.6 us
    all_to_all x1, blocking collectives, _apply_forms(): placed = jax.lax.all_to_all(piece_next, peer_axis, 0, 0)  32.7 us
    sub x1, other arithmetic, local(): signal_real = signal_real + all_re * h_re - all_im * h_im  19.2 us
    dynamic_slice x30, local copies, waits for them, and re-layouts, one(): lax.dynamic_index_in_dim(a, lap, 0, False)  13.7 us
    unnamed x17, other arithmetic  12.3 us
    slice x1, local copies, waits for them, and re-layouts, within_blocks(): new_re = step_re * h_re - step_im * h_im + blocks_re[:, offset]  9.73 us
    sub x2, local copies, waits for them, and re-layouts, local(): signal_real = local_re + inner_re * enter_re - inner_im * enter_im  7.41 us
  transfers between devices with their start and end apart: 2, of which 0 were waited for; matrix products, arithmetic and copies ran while one was open for 49% of the time, Pallas kernels for 0%

profile of v1, /device:TPU:31, one launch (start us, length us, event | category | flops | bytes accessed | tf_op | source)
XLA Modules:
  0.0 345.6 jit_solution(6687949648943361616)
XLA Ops:
  9.6 2.3 convolution_bitcast_fusion.1
  14.4 6.0 %copy.90 = f32[256,32,64]{2,1,0:T(8,128)} copy(f32[256,32,64]{0,2,1:T(8,128)} %convolution_bitcast_fusion.1) | data formatting | bytes 4194304 | tf_op jit(solution)/shard_map/sgc,gpc->sgp/transpose | solution.py:128
  20.5 5.2 %reshape_reshape.6 = f32[16,16,2048]{2,1,0:T(8,128)} reshape(f32[256,32,64]{2,1,0:T(8,128)} %copy.90) | data formatting | bytes 4194304 | tf_op jit(solution)/shard_map/reshape;reshape | solution.py:69
  25.7 9.7 %fusion.35 = (f32[16,1,2048]{2,1,0:T(1,128)}, f32[16,1,2048]{2,1,0:T(1,128)S(1)}, f32[16,1,2048]{2,1,0:T(1,128)}, f32[16,1,2048]{2,1,0:T(1,128)}, f32[16,1,2048]...) fusion(f32[16,16,2048]{2,1,0:T(8,128)} %reshape_reshape.6), kind=kLoop, calls=%fused_computation.173 | loop fusion | bytes 4194304 | tf_op jit(solution)/shard_map/slice | solution.py:76
  35.4 4.5 %copy.92 = f32[256,32,64]{2,1,0:T(8,128)} copy(f32[256,32,64]{0,2,1:T(8,128)S(1)} %convolution_bitcast_fusion) | data formatting | bytes 4194304 | tf_op jit(solution)/shard_map/sgc,gpc->sgp/transpose | solution.py:131
  39.9 3.6 %reshape_reshape.7 = f32[16,16,2048]{2,1,0:T(8,128)S(1)} reshape(f32[256,32,64]{2,1,0:T(8,128)} %copy.92) | data formatting | bytes 4194304 | tf_op jit(solution)/shard_map/reshape;reshape | solution.py:70
  43.6 1.6 fusion.34
  49.0 48.5 %while.33 = (s32[]{:T(128)}, f32[2048]{0:T(1024)S(1)}, f32[2048]{0:T(1024)S(1)}, f32[16,2048]{1,0:T(8,128)}, f32[16,2048]{1,0:T(8,128)}, /*index=5*/f32[2048]{0:...) while((s32[]{:T(128)}, f32[2048]{0:T(1024)S(1)}, ...), condition=%wide.region_1.2_spmd.clone, body=%wide.region_0.1_spmd.clone.sunk | while | flops 20483 | bytes 180355 | solution.py:93
  97.6 28.9 %all-gather = f32[32768]{0:T(1024)S(1)} all-gather(f32[2048]{0:T(1024)S(1)} %get-tuple-element.127), channel_id=2, replica_groups=mesh['sp'=16,'tp'=2] {'sp'}, dimensions={0}, use_global_device_ids=true | all-gather | bytes 139264 | tf_op jit(solution)/shard_map/all_gather | solution.py:22
  126.6 31.3 %all-gather.1 = f32[32768]{0:T(1024)S(1)} all-gather(f32[2048]{0:T(1024)S(1)} %get-tuple-element.128), channel_id=3, replica_groups=mesh['sp'=16,'tp'=2] {'sp'}, dimensions={0}, use_global_device_ids=true | all-gather | bytes 139264 | tf_op jit(solution)/shard_map/all_gather | solution.py:22
  158.0 29.2 %all-gather.3 = f32[16,1,2048]{2,1,0:T(1,128)S(1)} all-gather(f32[1,1,2048]{2,1,0:T(1,128)S(1)} %reshape.5974), channel_id=1, replica_groups=mesh['sp'=16,'tp'=2] {'sp'}, dimensions={0}, use_global_device_ids=true | all-gather | bytes 139264 | tf_op jit(solution)/shard_map/all_gather | solution.py:22
  188.0 30.9 %all-gather.2 = f32[16,1,2048]{2,1,0:T(1,128)S(1)} all-gather(f32[1,1,2048]{2,1,0:T(1,128)S(1)} %reshape.5972), channel_id=1, replica_groups=mesh['sp'=16,'tp'=2] {'sp'}, dimensions={0}, use_global_device_ids=true | all-gather | bytes 139264 | tf_op jit(solution)/shard_map/all_gather | solution.py:22
  219.6 14.7 %while.32 = (s32[]{:T(128)}, f32[2048]{0:T(1024)S(1)}, f32[2048]{0:T(1024)S(1)}, s32[]{:T(128)}, f32[16,2048]{1,0:T(8,128)}, /*index=5*/f32[16,2048]{1,0:T(8,128...) while((s32[]{:T(128)}, f32[2048]{0:T(1024)S(1)}, ...), condition=%wide.region_3.4_spmd, body=%wide.region_2.3_spmd.sunk | while | flops 16389 | bytes 131223 | solution.py:30
  248.3 2.8 multiply_subtract_fusion.1
  251.2 2.5 copy.126
  253.7 4.9 %add.1212 = f32[256,32,64]{2,1,0:T(8,128)} reshape(f32[16,16,2048]{2,1,0:T(8,128)} %copy.126) | data formatting | bytes 4194304 | tf_op jit(solution)/shard_map/add | solution.py:143
  258.6 2.5 copy.124
  261.1 4.9 %sub.375 = f32[256,32,64]{2,1,0:T(8,128)} reshape(f32[16,16,2048]{2,1,0:T(8,128)} %copy.124) | data formatting | bytes 4194304 | tf_op jit(solution)/shard_map/sub | solution.py:142
  266.0 19.2 %multiply_subtract_fusion = (f32[256,32,64]{2,1,0:T(8,128)S(1)}, f32[256,32,64]{2,1,0:T(8,128)S(1)}) fusion(f32[256,32,64]{2,1,0:T(8,128)} %sub.375, f32[32,64]{1,0:T(8,128)S(1)} %mul.2004, f32[32,64]{1,0:T(8,128)S(1)} %mul.2000, f32[32,64]{1,0:T(8,128)S(1)} %copy-done.52, f32[32,64]{1,0:T(8,128)S(1)} %copy-done.54, f32[256]{0:T(256)S(1)} %add_convert_fusion, ...), kind=kLoop, calls=%fused_computation.21 | loop fusion | flops 6291456 | bytes 8422400 | tf_op jit(solution)/shard_map/sub | solution.py:149
  285.2 6.1 %fusion.2 = f32[32,256,16]{1,2,0:T(8,128)S(1)} fusion(f32[32,16,64]{2,1,0:T(8,128)S(1)} %copy-done, f32[256,32,64]{2,1,0:T(8,128)S(1)} %get-tuple-element.315), kind=kOutput, calls=%fused_computation.16 | convolution fusion | flops 100663296 | bytes 2752512 | tf_op jit(solution)/shard_map/qej,eoj->qeo/dot_general | solution.py:155
  291.4 6.1 %fusion.6 = f32[32,256,16]{1,2,0:T(8,128)S(1)} fusion(f32[32,256,16]{1,2,0:T(8,128)S(1)} %fusion.2, f32[32,16,64]{2,1,0:T(8,128)S(1)} %copy-done.50, f32[256,32,64]{2,1,0:T(8,128)S(1)} %get-tuple-element.314), kind=kOutput, calls=%fused_computation.31 | convolution fusion | flops 100794368 | bytes 3276800 | tf_op jit(solution)/shard_map/qej,eoj->qeo/dot_general | solution.py:153
  298.0 32.7 %all_to_all.5 = bf16[2,128,512]{2,1,0:T(8,128)(2,1)S(1)} all-to-all(bf16[2,128,512]{2,1,0:T(8,128)(2,1)S(1)} %pad_maximum_fusion), channel_id=1, replica_groups=mesh['sp'=16,'tp'=2] {'tp'}, dimensions={0} | all-to-all | bytes 524288 | tf_op jit(solution)/shard_map/all_to_all | solution.py:13
  330.7 2.9 convolution_convert_fusion.1
  333.8 2.9 convolution_convert_fusion
  (322 shorter events, 88.9 us)
Async XLA Ops:
  6.5 278.7 %copy-start = (f32[32,16,64]{2,1,0:T(8,128)S(1)}, f32[32,16,64]{2,1,0:T(8,128)}, u32[]{:S(2)}) copy-start(f32[32,16,64]{2,1,0:T(8,128)} %param.24) | copy-start | bytes 393220
  6.6 324.1 %all-gather.7.cloned.1.call-start = ((), (), s32[]{:S(2)}) async-start(), calls=%async_computation.1 | async-start | bytes 6291456 | tf_op jit(solution)/shard_map/all_gather | solution.py:161
  7.3 326.5 %all-gather.9.cloned.1.call-start = ((), (), s32[]{:S(2)}) async-start(), calls=%async_computation.2 | async-start | bytes 6291456 | tf_op jit(solution)/shard_map/all_gather | solution.py:162
  9.6 3.4 copy-start.53
  9.6 4.1 %copy-start.51 = (f32[32,64]{1,0:T(8,128)}, f32[32,64]{1,0:T(8,128)S(1)}, u32[]{:S(2)}) copy-start(f32[32,64]{1,0:T(8,128)S(1)} %get-tuple-element.320) | copy-start | bytes 24580
  43.6 3.5 %copy-start.15 = (f32[16,1,2048]{2,1,0:T(1,128)S(1)}, f32[16,1,2048]{2,1,0:T(1,128)}, u32[]{:S(2)}) copy-start(f32[16,1,2048]{2,1,0:T(1,128)} %get-tuple-element.281) | copy-start | bytes 393220
  43.6 3.5 %copy-start.19 = (f32[16,1,2048]{2,1,0:T(1,128)S(1)}, f32[16,1,2048]{2,1,0:T(1,128)}, u32[]{:S(2)}) copy-start(f32[16,1,2048]{2,1,0:T(1,128)} %get-tuple-element.283) | copy-start | bytes 393220
  43.6 3.5 %copy-start.23 = (f32[16,1,2048]{2,1,0:T(1,128)S(1)}, f32[16,1,2048]{2,1,0:T(1,128)}, u32[]{:S(2)}) copy-start(f32[16,1,2048]{2,1,0:T(1,128)} %get-tuple-element.284) | copy-start | bytes 393220
  48.2 109.7 %copy-start.58 = (f32[32,64]{1,0:T(8,128)S(1)}, f32[32,64]{1,0:T(8,128)}, u32[]{:S(2)}) copy-start(f32[32,64]{1,0:T(8,128)} %get-tuple-element.316) | copy-start | bytes 24580
  48.8 139.1 %copy-start.57 = (f32[32,64]{1,0:T(8,128)S(1)}, f32[32,64]{1,0:T(8,128)}, u32[]{:S(2)}) copy-start(f32[32,64]{1,0:T(8,128)} %get-tuple-element.317) | copy-start | bytes 24580
  49.0 185.3 %copy-start.41 = (f32[16,1,2048]{2,1,0:T(1,128)S(1)}, f32[16,1,2048]{2,1,0:T(1,128)}, u32[]{:S(2)}) copy-start(f32[16,1,2048]{2,1,0:T(1,128)} %get-tuple-element.287) | copy-start | bytes 393220
  49.0 186.1 %copy-start.35 = (f32[16,1,2048]{2,1,0:T(1,128)S(1)}, f32[16,1,2048]{2,1,0:T(1,128)}, u32[]{:S(2)}) copy-start(f32[16,1,2048]{2,1,0:T(1,128)} %get-tuple-element.286) | copy-start | bytes 393220
  49.0 186.1 %copy-start.39 = (f32[16,1,2048]{2,1,0:T(1,128)S(1)}, f32[16,1,2048]{2,1,0:T(1,128)}, u32[]{:S(2)}) copy-start(f32[16,1,2048]{2,1,0:T(1,128)} %copy-done.38) | copy-start | bytes 393220
  126.5 109.5 %copy-start.31 = (f32[16,1,2048]{2,1,0:T(1,128)S(1)}, f32[16,1,2048]{2,1,0:T(1,128)}, u32[]{:S(2)}) copy-start(f32[16,1,2048]{2,1,0:T(1,128)} %get-tuple-element.285) | copy-start | bytes 393220
  126.6 109.5 %copy-start.37 = (f32[16,1,2048]{2,1,0:T(1,128)S(1)}, f32[16,1,2048]{2,1,0:T(1,128)}, u32[]{:S(2)}) copy-start(f32[16,1,2048]{2,1,0:T(1,128)} %copy-done.36) | copy-start | bytes 393220
  219.6 17.3 %copy-start.24 = (f32[16,1,2048]{2,1,0:T(1,128)S(1)}, f32[16,1,2048]{2,1,0:T(1,128)}, u32[]{:S(2)}) copy-start(f32[16,1,2048]{2,1,0:T(1,128)} %get-tuple-element.284) | copy-start | bytes 393220
  219.6 17.3 %copy-start.33 = (f32[16,1,2048]{2,1,0:T(1,128)S(1)}, f32[16,1,2048]{2,1,0:T(1,128)}, u32[]{:S(2)}) copy-start(f32[16,1,2048]{2,1,0:T(1,128)} %copy-done.32) | copy-start | bytes 393220
  244.3 4.0 %copy-start.47 = (f32[16,2048]{1,0:T(8,128)S(1)}, f32[16,2048]{1,0:T(8,128)}, u32[]{:S(2)}) copy-start(f32[16,2048]{1,0:T(8,128)} %copy-done.46) | copy-start | bytes 393220
  244.3 4.0 %copy-start.49 = (f32[16,2048]{1,0:T(8,128)S(1)}, f32[16,2048]{1,0:T(8,128)}, u32[]{:S(2)}) copy-start(f32[16,2048]{1,0:T(8,128)} %copy-done.48) | copy-start | bytes 393220
  261.1 4.9 %copy-start.52 = (f32[32,64]{1,0:T(8,128)S(1)}, f32[32,64]{1,0:T(8,128)}, u32[]{:S(2)}) copy-start(f32[32,64]{1,0:T(8,128)} %copy-done.51) | copy-start | bytes 24580
  261.1 4.9 %copy-start.54 = (f32[32,64]{1,0:T(8,128)S(1)}, f32[32,64]{1,0:T(8,128)}, u32[]{:S(2)}) copy-start(f32[32,64]{1,0:T(8,128)} %copy-done.53) | copy-start | bytes 24580
  285.2 6.1 %copy-start.50 = (f32[32,16,64]{2,1,0:T(8,128)S(1)}, f32[32,16,64]{2,1,0:T(8,128)}, u32[]{:S(2)}) copy-start(f32[32,16,64]{2,1,0:T(8,128)} %param.23) | copy-start | bytes 393220
  291.3 6.3 %copy-start.45 = (bf16[256,512]{1,0:T(8,128)(2,1)S(1)}, bf16[256,512]{1,0:T(8,128)(2,1)}, u32[]{:S(2)}) copy-start(bf16[256,512]{1,0:T(8,128)(2,1)} %param.17) | copy-start | bytes 786436
  291.3 6.3 %copy-start.65 = (f32[512]{0:T(512)S(1)}, f32[512]{0:T(512)}, u32[]{:S(2)}) copy-start(f32[512]{0:T(512)} %param.25) | copy-start | bytes 6148
  (46 other events, 113.1 us)
Sparse Core Ops, SparseCore 0:
  8.9 15.2 all-gather.6
  25.8 14.8 all-gather.8
